TPU v7x, 512 devices: a 4x2x32 block of a 4x8x32 slice. The times are simulated.
512 devices in a mesh: grp: 2 (over y), sp: 64 (over z, core), tp: 4 (over x).
Axes of the slice: x: 4, y: 2, z: 32, core: 2. Of those that a mesh axis runs over, the one named last changes fastest.
The devices are a block of a 4x8x32 slice.
Arguments:
- tokens: bfloat16 [131072, 2048], P(('grp', 'sp', 'tp')), parts along dimension 0, may hold values from -6 to 6
- step: float32 [131072], P(('grp', 'sp')), parts along dimension 0, may hold values from 0.2 to 3.75
- in_gain: float32 [2048], replicated, may hold values from 0.1 to 1.9
- in_proj: bfloat16 [2048, 512], P(None, 'tp'), may hold values from -0.125 to 0.125
- decay_rate: float32 [32, 64], P('tp'), may hold values from 1.5258789e-06 to 0.04
- frequency: float32 [32, 64], P('tp'), may hold values from 0.2 to 3
- input_map: float32 [2, 32, 64, 16], P(None, 'tp'), may hold values from -1 to 1
- readout: float32 [2, 32, 16, 64], P(None, 'tp'), may hold values from -0.75 to 0.75
- out_gain: float32 [512], replicated, may hold values from 0.1 to 1.9
- out_proj: bfloat16 [512, 2048], replicated, may hold values from -0.25 to 0.25
Outputs:
- mixed: bfloat16 [131072, 2048], P(('grp', 'sp', 'tp')), parts along dimension 0
There are 2 independent parts, one for each index of `grp`. A program takes and returns all parts, laid end to end along the dimension named above; an argument that names none is the same for every part. Nothing has to cross between parts.
All inputs are finite; a program needn't handle non-finite values.
Results may differ from a plain program's by a relative error of at most 0.01.
Values may be sent and summed in bfloat16 or wider, within the bound.
No kernel may reach another device: no remote copies, remote signals or barrier semaphores. Data moves between devices by JAX's collectives and lax.ppermute only.
A program may use at most 64 MiB of HBM per device.

v0:
```python
from functools import partial
import jax
import jax.numpy as jnp
from jax import lax
from jax.sharding import PartitionSpec as P

SPAN = 64
HIGHEST = lax.Precision.HIGHEST


def gathered_once(array, axis):
    leaves = jax.tree.leaves(array)
    sequence = sorted(range(len(leaves)), key=lambda k: -leaves[k].size)
    width = (1, *leaves[sequence[0]].shape)[-1]
    lines = [
        jnp.pad(leaves[k].reshape(-1), (0, -leaves[k].size % width)).reshape(-1, width)
        for k in sequence
    ]
    both, at, found = (lax.all_gather(jnp.concatenate(lines), axis), 0, {})
    for k, line in zip(sequence, lines):
        section = both[:, at : at + len(line)].reshape(len(both), -1)
        found[k] = section[:, : leaves[k].size].reshape(-1, *leaves[k].shape)
        at += len(line)
    numbers = iter(range(len(leaves)))
    return jax.tree.map(lambda _: found[next(numbers)], array)


def entering(value, axis, join, neutral):
    count, mine = (lax.axis_size(axis), lax.axis_index(axis))
    pieces = gathered_once(value, axis)
    so_far = jax.tree.map(
        lambda part, zero: jnp.full_like(part, 0) + jnp.asarray(zero, part.dtype), value, neutral
    )

    def lap(position, so_far):
        longer = join(so_far, jax.tree.map(lambda part: part[position], pieces))
        return jax.tree.map(lambda new, old: jnp.where(position < mine, new, old), longer, so_far)

    return lax.fori_loop(0, count - 1, lap, so_far)


def compose(earlier, later):
    a_re, a_im, b_re, b_im = earlier
    c_re, c_im, d_re, d_im = later
    return (
        c_re * a_re - c_im * a_im,
        c_re * a_im + c_im * a_re,
        c_re * b_re - c_im * b_im + d_re,
        c_re * b_im + c_im * b_re + d_im,
    )


def rms_rows(values, gain):
    values = values.astype(jnp.float32)
    scaled = values * lax.rsqrt(jnp.mean(values * values, axis=-1, keepdims=True) + 1e-06)
    return (scaled * gain).astype(jnp.bfloat16)


def block_tables(input_map, readout):
    groups = input_map.shape[1]
    unit = jnp.eye(groups, dtype=jnp.float32)
    push_re = jnp.einsum("gph,gk->ghkp", input_map[0], unit, precision=HIGHEST)
    push_im = jnp.einsum("gph,gk->ghkp", input_map[1], unit, precision=HIGHEST)
    read_re = jnp.einsum("ghp,gk->gpkh", readout[0], unit, precision=HIGHEST)
    read_im = jnp.einsum("ghp,gk->gpkh", readout[1], unit, precision=HIGHEST)
    inner = push_re.shape[0] * push_re.shape[1]
    flat = push_re.shape[2] * push_re.shape[3]
    return (
        push_re.reshape(inner, flat),
        push_im.reshape(inner, flat),
        read_re.reshape(flat, inner),
        read_im.reshape(flat, inner),
    )


def response(s_re, s_im, read_re, read_im):
    value = jnp.dot(s_re, read_re, precision=HIGHEST) - jnp.dot(s_im, read_im, precision=HIGHEST)
    return jax.nn.gelu(value, approximate=True).astype(jnp.bfloat16)


def advance(carry, piece, rates, freqs, tables, lower, keep):
    drive_part, time_part = piece
    push_re, push_im, read_re, read_im = tables
    own = time_part[:, None]
    magnitude = jnp.exp(-rates[None] * own)
    a_re = magnitude * jnp.cos(freqs[None] * own)
    a_im = magnitude * jnp.sin(freqs[None] * own)
    lam_re = -rates
    denom = lam_re * lam_re + freqs * freqs
    n_re = a_re - 1.0
    z_re = (n_re * lam_re + a_im * freqs) / denom
    z_im = (a_im * lam_re - n_re * freqs) / denom
    grouped = drive_part.astype(jnp.float32)
    in_re = jnp.dot(grouped, push_re, precision=HIGHEST)
    in_im = jnp.dot(grouped, push_im, precision=HIGHEST)
    i_re = z_re * in_re - z_im * in_im
    i_im = z_re * in_im + z_im * in_re
    elapsed = jnp.dot(lower, time_part, precision=HIGHEST)[:, None]
    grow = jnp.exp(rates[None] * elapsed)
    angle = freqs[None] * elapsed
    cosine = jnp.cos(angle)
    sine = jnp.sin(angle)
    w_re = grow * (cosine * i_re + sine * i_im)
    w_im = grow * (cosine * i_im - sine * i_re)
    acc_re = jnp.dot(lower, w_re, precision=HIGHEST)
    acc_im = jnp.dot(lower, w_im, precision=HIGHEST)
    shrink = jnp.exp(-rates[None] * elapsed)
    c_re = shrink * cosine
    c_im = shrink * sine
    s_re = c_re * acc_re - c_im * acc_im
    s_im = c_re * acc_im + c_im * acc_re
    d_re, d_im, e_re, e_im = carry
    full_re = s_re + c_re * e_re - c_im * e_im
    full_im = s_im + c_re * e_im + c_im * e_re
    cum_re = c_re * d_re - c_im * d_im
    cum_im = c_re * d_im + c_im * d_re
    ends = (cum_re[-1], cum_im[-1], full_re[-1], full_im[-1])
    return (ends, (cum_re, cum_im, full_re, full_im))


def on_device(
    tokens, step, in_gain, in_proj, decay_rate, frequency, input_map, readout, out_gain, out_proj
):
    normed = rms_rows(tokens, in_gain)
    rates, freqs, maps, reads = (decay_rate, frequency, input_map, readout)
    drive = jnp.dot(
        lax.all_gather(normed, "tp", axis=0, tiled=True),
        in_proj,
        preferred_element_type=jnp.float32,
    ).astype(jnp.bfloat16)
    tables = block_tables(maps, reads)
    flat_rates = rates.reshape(-1)
    flat_freqs = freqs.reshape(-1)
    seq_rows = drive.shape[0]
    block_count = seq_rows // SPAN
    drive_blocks = drive.reshape(block_count, SPAN, -1)
    time_blocks = step.reshape(block_count, SPAN)
    rows_index = lax.broadcasted_iota(jnp.int32, (SPAN, SPAN), 0)
    cols_index = lax.broadcasted_iota(jnp.int32, (SPAN, SPAN), 1)
    lower = (cols_index <= rows_index).astype(jnp.float32)
    zeros = jnp.zeros(flat_rates.shape, jnp.float32)
    ones = jnp.ones(flat_rates.shape, jnp.float32)
    start_carry = (ones, zeros, zeros, zeros)
    keep_first = "states"
    ends, stored = lax.scan(
        partial(
            advance, rates=flat_rates, freqs=flat_freqs, tables=tables, lower=lower, keep=keep_first
        ),
        start_carry,
        (drive_blocks, time_blocks),
    )
    incoming = entering(ends, "sp", compose, start_carry)
    cum_re, cum_im, full_re, full_im = stored
    width = flat_rates.shape[0]
    cum_re = cum_re.reshape(seq_rows, width)
    cum_im = cum_im.reshape(seq_rows, width)
    state_re = full_re.reshape(seq_rows, width) + cum_re * incoming[2] - cum_im * incoming[3]
    state_im = full_im.reshape(seq_rows, width) + cum_re * incoming[3] + cum_im * incoming[2]
    answer = response(state_re, state_im, tables[2], tables[3])
    gathered = lax.all_to_all(answer, "tp", split_axis=0, concat_axis=1, tiled=True)
    shaped = rms_rows(gathered, out_gain)
    return jnp.dot(shaped, out_proj, preferred_element_type=jnp.float32).astype(jnp.bfloat16)


def solution(mesh):
    placed = (
        P(("grp", "sp", "tp"), None),
        P(("grp", "sp")),
        P(),
        P(None, "tp"),
        P("tp", None),
        P("tp", None),
        P(None, "tp", None, None),
        P(None, "tp", None, None),
        P(),
        P(),
    )
    return jax.shard_map(
        on_device,
        mesh=mesh,
        in_specs=placed,
        out_specs=P(("grp", "sp", "tp"), None),
        check_vma=False,
    )
```

profile of v0, /device:TPU:33, one launch (start us, length us, event | category | flops | bytes accessed | tf_op | source)
XLA Modules:
  0.0 373.2 jit_solution(620879934638658215)
XLA Ops:
  8.3 2.5 fusion.46
  15.7 85.1 %all-gather.4.cloned.1.call-done = bf16[1024,2048]{1,0:T(8,128)(2,1)} async-done(((bf16[256,2048]{1,0:T(8,128)(2,1)}), bf16[1024,2048]{1,0:T(8,128)(2,1)}) %all-gather.4.cloned.1.call-update) | async-done | bytes 4194320 | tf_op jit(solution)/shard_map/all_gather | solution.py:127
  100.8 4.3 %convolution_convert_fusion.1 = bf16[1024,128]{1,0:T(8,128)(2,1)} fusion(bf16[1024,2048]{1,0:T(8,128)(2,1)} %all-gather.4.cloned.1.call-done, bf16[2048,128]{1,0:T(8,128)(2,1)} %param.17), kind=kOutput, calls=%fused_computation.81 | convolution fusion | flops 537001984 | bytes 4980736 | tf_op jit(solution)/shard_map/dot_general | solution.py:126
  106.2 173.9 %while.48 = (s32[]{:T(128)}, f32[512]{0:T(512)S(1)}, f32[512]{0:T(512)S(1)}, f32[512]{0:T(512)}, f32[512]{0:T(512)}, /*index=5*/f32[16,64,512]{2,1,0:T(8,128)}, ...) while((s32[]{:T(128)}, f32[512]{0:T(512)S(1)}, ...), condition=%wide.wide.region_2.3_spmd.clone.clone.clone, body=%wide.wide.region_1.2_spmd.clone.clone.clone.sunk | while | flops 153889792 | bytes 4405837 | solution.py:145
  112.3 3.0 add_dynamic-update-slice_fusion.3
  123.2 3.0 add_dynamic-update-slice_fusion.3
  134.1 3.0 add_dynamic-update-slice_fusion.3
  144.9 3.0 add_dynamic-update-slice_fusion.3
  155.8 3.0 add_dynamic-update-slice_fusion.3
  166.7 3.0 add_dynamic-update-slice_fusion.3
  177.6 3.0 add_dynamic-update-slice_fusion.3
  188.4 3.0 add_dynamic-update-slice_fusion.3
  199.3 3.0 add_dynamic-update-slice_fusion.3
  210.2 3.0 add_dynamic-update-slice_fusion.3
  221.0 3.0 add_dynamic-update-slice_fusion.3
  231.9 3.0 add_dynamic-update-slice_fusion.3
  242.8 3.0 add_dynamic-update-slice_fusion.3
  253.6 3.0 add_dynamic-update-slice_fusion.3
  264.5 3.0 add_dynamic-update-slice_fusion.3
  275.4 3.0 add_dynamic-update-slice_fusion.3
  280.9 60.4 %all-gather.1 = f32[64,4,512]{2,1,0:T(4,128)S(1)} all-gather(f32[1,4,512]{2,1,0:T(4,128)S(1)} %maximum_bitcast_fusion), channel_id=2, replica_groups=mesh['grp'=2,'sp'=64,'tp'=4] {'sp'}, dimensions={0}, use_global_device_ids=true | all-gather | bytes 532480 | tf_op jit(solution)/shard_map/all_gather | solution.py:19
  341.7 5.1 %while.47 = (s32[]{:T(128)}, f32[512]{0:T(512)S(1)}, f32[512]{0:T(512)S(1)}, s32[]{:T(128)}, f32[64,512]{1,0:T(8,128)S(1)}, /*index=5*/f32[64,512]{1,0:T(8,128)S...) while((s32[]{:T(128)}, f32[512]{0:T(512)S(1)}, f32[512]{0:T(512)S(1)}, ...), condition=%wide.region_4.5_spmd.clone, body=%wide.region_3.4_spmd.clone.sunk | while | flops 6148 | bytes 32897 | solution.py:39
  346.8 4.6 %multiply_add_fusion.5 = (f32[16,64,512]{2,1,0:T(8,128)S(1)}, f32[16,64,512]{2,1,0:T(8,128)S(1)}) fusion(f32[16,64,512]{2,1,0:T(8,128)} %get-tuple-element.435, f32[16,64,512]{2,1,0:T(8,128)} %get-tuple-element.437, f32[16,64,512]{2,1,0:T(8,128)} %get-tuple-element.429, f32[512]{0:T(512)S(1)} %get-tuple-element.436, f32[512]{0:T(512)S(1)} %get-tuple-element.434, ...), kind=kLoop, calls=%fused_computation.78 | loop fusion | flops 4194304 | bytes 12587008 | tf_op jit(solution)/shard_map/add | solution.py:158
  355.2 9.2 %all_to_all.13 = bf16[4,256,128]{1,2,0:T(8,128)(2,1)S(1)} all-to-all(bf16[4,256,128]{1,2,0:T(8,128)(2,1)S(1)} %copy.20), channel_id=1, replica_groups=mesh['grp'=2,'sp'=64,'tp'=4] {'tp'}, dimensions={0} | all-to-all | bytes 524288 | tf_op jit(solution)/shard_map/all_to_all | solution.py:160
  (635 shorter events, 140.3 us)
Async XLA Ops:
  6.5 358.1 %copy-start = (bf16[512,2048]{1,0:T(8,128)(2,1)S(1)}, bf16[512,2048]{1,0:T(8,128)(2,1)}, u32[]{:S(2)}) copy-start(bf16[512,2048]{1,0:T(8,128)(2,1)} %param.23) | copy-start | bytes 6291460
  6.6 6.4 %copy-start.12 = (f32[1024]{0:T(1024)S(1)}, f32[1024]{0:T(1024)}, u32[]{:S(2)}) copy-start(f32[1024]{0:T(1024)} %param.15) | copy-start | bytes 12292
  6.6 7.0 %copy-start.3 = (f32[2,8,16,64]{3,2,1,0:T(8,128)S(1)}, f32[2,8,16,64]{3,2,1,0:T(8,128)}, u32[]{:S(2)}) copy-start(f32[2,8,16,64]{3,2,1,0:T(8,128)} %param.21) | copy-start | bytes 196612
  6.6 94.2 %all-gather.4.cloned.1.call-start = ((), (), s32[]{:S(2)}) async-start(), calls=%async_computation.1 | async-start | bytes 5242880 | tf_op jit(solution)/shard_map/all_gather | solution.py:127
  128.3 5.7 %copy-start.5 = (f32[1,512]{1,0:T(1,128)S(1)}, f32[1,512]{1,0:T(1,128)}, u32[]{:S(2)}) copy-start(f32[1,512]{1,0:T(1,128)} %get-tuple-element.1028) | copy-start | bytes 6148 | tf_op jit(solution)/shard_map/while
  128.3 5.7 %copy-start.10 = (f32[512]{0:T(512)S(1)}, f32[512]{0:T(512)}, u32[]{:S(2)}) copy-start(f32[512]{0:T(512)} %get-tuple-element.1001) | copy-start | bytes 6148 | tf_op jit(solution)/shard_map/while
  128.3 5.7 %copy-start.11 = (f32[512]{0:T(512)S(1)}, f32[512]{0:T(512)}, u32[]{:S(2)}) copy-start(f32[512]{0:T(512)} %get-tuple-element.1002) | copy-start | bytes 6148 | tf_op jit(solution)/shard_map/while
  128.3 5.7 %copy-start.14 = (f32[512]{0:T(512)S(1)}, f32[512]{0:T(512)}, u32[]{:S(2)}) copy-start(f32[512]{0:T(512)} %get-tuple-element.1038) | copy-start | bytes 6148 | tf_op jit(solution)/shard_map/while
  128.3 5.7 %copy-start.15 = (f32[1,512]{1,0:T(1,128)S(1)}, f32[1,512]{1,0:T(1,128)}, u32[]{:S(2)}) copy-start(f32[1,512]{1,0:T(1,128)} %get-tuple-element.1032) | copy-start | bytes 6148 | tf_op jit(solution)/shard_map/while
  139.1 5.7 %copy-start.5 = (f32[1,512]{1,0:T(1,128)S(1)}, f32[1,512]{1,0:T(1,128)}, u32[]{:S(2)}) copy-start(f32[1,512]{1,0:T(1,128)} %get-tuple-element.1028) | copy-start | bytes 6148 | tf_op jit(solution)/shard_map/while
  139.2 5.7 %copy-start.10 = (f32[512]{0:T(512)S(1)}, f32[512]{0:T(512)}, u32[]{:S(2)}) copy-start(f32[512]{0:T(512)} %get-tuple-element.1001) | copy-start | bytes 6148 | tf_op jit(solution)/shard_map/while
  139.2 5.7 %copy-start.11 = (f32[512]{0:T(512)S(1)}, f32[512]{0:T(512)}, u32[]{:S(2)}) copy-start(f32[512]{0:T(512)} %get-tuple-element.1002) | copy-start | bytes 6148 | tf_op jit(solution)/shard_map/while
  139.2 5.7 %copy-start.14 = (f32[512]{0:T(512)S(1)}, f32[512]{0:T(512)}, u32[]{:S(2)}) copy-start(f32[512]{0:T(512)} %get-tuple-element.1038) | copy-start | bytes 6148 | tf_op jit(solution)/shard_map/while
  139.2 5.7 %copy-start.15 = (f32[1,512]{1,0:T(1,128)S(1)}, f32[1,512]{1,0:T(1,128)}, u32[]{:S(2)}) copy-start(f32[1,512]{1,0:T(1,128)} %get-tuple-element.1032) | copy-start | bytes 6148 | tf_op jit(solution)/shard_map/while
  150.0 5.7 %copy-start.5 = (f32[1,512]{1,0:T(1,128)S(1)}, f32[1,512]{1,0:T(1,128)}, u32[]{:S(2)}) copy-start(f32[1,512]{1,0:T(1,128)} %get-tuple-element.1028) | copy-start | bytes 6148 | tf_op jit(solution)/shard_map/while
  150.0 5.7 %copy-start.10 = (f32[512]{0:T(512)S(1)}, f32[512]{0:T(512)}, u32[]{:S(2)}) copy-start(f32[512]{0:T(512)} %get-tuple-element.1001) | copy-start | bytes 6148 | tf_op jit(solution)/shard_map/while
  150.0 5.7 %copy-start.11 = (f32[512]{0:T(512)S(1)}, f32[512]{0:T(512)}, u32[]{:S(2)}) copy-start(f32[512]{0:T(512)} %get-tuple-element.1002) | copy-start | bytes 6148 | tf_op jit(solution)/shard_map/while
  150.0 5.7 %copy-start.14 = (f32[512]{0:T(512)S(1)}, f32[512]{0:T(512)}, u32[]{:S(2)}) copy-start(f32[512]{0:T(512)} %get-tuple-element.1038) | copy-start | bytes 6148 | tf_op jit(solution)/shard_map/while
  150.1 5.7 %copy-start.15 = (f32[1,512]{1,0:T(1,128)S(1)}, f32[1,512]{1,0:T(1,128)}, u32[]{:S(2)}) copy-start(f32[1,512]{1,0:T(1,128)} %get-tuple-element.1032) | copy-start | bytes 6148 | tf_op jit(solution)/shard_map/while
  160.9 5.7 %copy-start.5 = (f32[1,512]{1,0:T(1,128)S(1)}, f32[1,512]{1,0:T(1,128)}, u32[]{:S(2)}) copy-start(f32[1,512]{1,0:T(1,128)} %get-tuple-element.1028) | copy-start | bytes 6148 | tf_op jit(solution)/shard_map/while
  160.9 5.7 %copy-start.10 = (f32[512]{0:T(512)S(1)}, f32[512]{0:T(512)}, u32[]{:S(2)}) copy-start(f32[512]{0:T(512)} %get-tuple-element.1001) | copy-start | bytes 6148 | tf_op jit(solution)/shard_map/while
  280.2 61.5 %copy-start.6 = (f32[512]{0:T(512)S(1)}, f32[512]{0:T(512)}, u32[]{:S(2)}) copy-start(f32[512]{0:T(512)} %custom-call) | copy-start | bytes 6148
  280.2 61.5 %copy-start.7 = (f32[512]{0:T(512)S(1)}, f32[512]{0:T(512)}, u32[]{:S(2)}) copy-start(f32[512]{0:T(512)} %custom-call.1) | copy-start | bytes 6148
  353.2 11.3 %copy-start.13 = (f32[512]{0:T(512)S(1)}, f32[512]{0:T(512)}, u32[]{:S(2)}) copy-start(f32[512]{0:T(512)} %param.22) | copy-start | bytes 6148
  (68 other events, 381.6 us)
Sparse Core Ops, SparseCore 0:
  11.0 89.7 all-gather.3
where the time goes:
time: 378 us; the launch traced here: 373 us
  matrix products  134 us (35%)
  waiting for transfers between devices  85.1 us (23%)
  blocking collectives  69.5 us (18%)
  local copies, waits for them, and re-layouts  43.1 us (11%)
  other arithmetic  22.5 us (6%)
  between operations  13.7 us (4%)
  loops' own time  5.22 us (1%)
    all_gather x1, waiting for transfers between devices, on_device(): lax.all_gather(normed, 'tp', axis=0, tiled=True)  85.1 us
    all_gather x1, blocking collectives, gathered_once(): both, at, found = (lax.all_gather(jnp.concatenate(lines), axis), 0, {})  60.4 us
    dot_general x16, matrix products, advance(): acc_im = jnp.dot(lower, w_im, precision=HIGHEST)  48.1 us
    dot_general x16, matrix products, advance(): acc_re = jnp.dot(lower, w_re, precision=HIGHEST)  32.4 us
    slice x32, local copies, waits for them, and re-layouts, advance(): ends = (cum_re[-1], cum_im[-1], full_re[-1], full_im[-1])  18.8 us
    dot_general x16, matrix products, advance(): in_im = jnp.dot(grouped, push_im, precision=HIGHEST)  15.3 us
    dot_general x16, matrix products, advance(): in_re = jnp.dot(grouped, push_re, precision=HIGHEST)  15.3 us
    dot_general x16, matrix products, advance(): elapsed = jnp.dot(lower, time_part, precision=HIGHEST)[:, None]  13.3 us
  transfers between devices with their start and end apart: 1, of which 1 were waited for; matrix products, arithmetic and copies ran while one was open for 1% of the time, Pallas kernels for 0%

commit v1 on v0

--- a/solution.py
+++ b/solution.py
@@ -6,6 +6,24 @@
 
 SPAN = 64
 HIGHEST = lax.Precision.HIGHEST
+
+
+def ring_gather(array, axis, dim):
+    ways, here, step = (lax.axis_size(axis), lax.axis_index(axis), array.shape[dim])
+    lengths = [n * ways if d == dim else n for d, n in enumerate(array.shape)]
+    full = lax.dynamic_update_slice_in_dim(
+        jnp.zeros(lengths, array.dtype), array, here * step, axis=dim
+    )
+    going_up = going_down = array
+    for far in range(1, ways // 2 + 1):
+        going_up = lax.ppermute(going_up, axis, [(d, (d + 1) % ways) for d in range(ways)])
+        full = lax.dynamic_update_slice_in_dim(full, going_up, (here - far) % ways * step, axis=dim)
+        if 2 * far < ways:
+            going_down = lax.ppermute(going_down, axis, [(d, (d - 1) % ways) for d in range(ways)])
+            full = lax.dynamic_update_slice_in_dim(
+                full, going_down, (here + far) % ways * step, axis=dim
+            )
+    return full
 
 
 def gathered_once(array, axis):
@@ -124,9 +142,7 @@
     normed = rms_rows(tokens, in_gain)
     rates, freqs, maps, reads = (decay_rate, frequency, input_map, readout)
     drive = jnp.dot(
-        lax.all_gather(normed, "tp", axis=0, tiled=True),
-        in_proj,
-        preferred_element_type=jnp.float32,
+        ring_gather(normed, "tp", 0), in_proj, preferred_element_type=jnp.float32
     ).astype(jnp.bfloat16)
     tables = block_tables(maps, reads)
     flat_rates = rates.reshape(-1)

time: 378 us -> 373 us (0.987)
  waiting for transfers between devices: 85.1 us -> 15.7 us
  blocking collectives: 69.5 us -> 119 us
  starting transfers between devices: 0.06 us -> 19.2 us
  between operations: 13.7 us -> 0.38 us
  local copies, waits for them, and re-layouts: 43.1 us -> 52.8 us
    all_gather x1 -> x0, waiting for transfers between devices: 85.1 us -> none  [on_device(): lax.all_gather(normed, 'tp', axis=0, tiled=True)]
    all_gather x1, blocking collectives: 60.4 us -> 110 us  [gathered_once(): both, at, found = (lax.all_gather(jnp.concatenate(lines), axis), 0, {})]
    ppermute x0 -> x3, starting transfers between devices: none -> 19.2 us  [the longest x2 15.7 us: ring_gather(): lax.ppermute(going_up, axis, [(d, (d + 1) % ways) for d in range(ways)])]
    ppermute x0 -> x3, waiting for transfers between devices: none -> 15.7 us  [the longest x2 15.7 us: ring_gather(): lax.ppermute(going_up, axis, [(d, (d + 1) % ways) for d in range(ways)])]
    dynamic_update_slice x0 -> x3, local copies, waits for them, and re-layouts: none -> 7.02 us  [the longest x2 4.66 us: ring_gather(): lax.dynamic_update_slice_in_dim(full, going_up, (here - far) % ways * ste...]
  transfers between devices with their start and end apart: 1 -> 3, of which waited for: 1 -> 2; matrix products, arithmetic and copies ran while one was open for 1% -> 3% of each run, Pallas kernels for 0% -> 0%
where the time goes in v1:
time: 373 us; the launch traced here: 369 us
  matrix products  134 us (36%)
  blocking collectives  119 us (32%)
  local copies, waits for them, and re-layouts  52.8 us (14%)
  other arithmetic  21.7 us (6%)
  starting transfers between devices  19.2 us (5%)
  waiting for transfers between devices  15.7 us (4%)
  loops' own time  5.22 us (1%)
    all_gather x1, blocking collectives, gathered_once(): both, at, found = (lax.all_gather(jnp.concatenate(lines), axis), 0, {})  110 us
    dot_general x16, matrix products, advance(): acc_im = jnp.dot(lower, w_im, precision=HIGHEST)  48 us
    dot_general x16, matrix products, advance(): acc_re = jnp.dot(lower, w_re, precision=HIGHEST)  33.2 us
    slice x32, local copies, waits for them, and re-layouts, advance(): ends = (cum_re[-1], cum_im[-1], full_re[-1], full_im[-1])  19 us
    ppermute x2, waiting for transfers between devices, ring_gather(): lax.ppermute(going_up, axis, [(d, (d + 1) % ways) for d in range(ways)])  15.7 us
    ppermute x2, starting transfers between devices, ring_gather(): lax.ppermute(going_up, axis, [(d, (d + 1) % ways) for d in range(ways)])  15.7 us
    dot_general x16, matrix products, advance(): in_im = jnp.dot(grouped, push_im, precision=HIGHEST)  15.3 us
    dot_general x16, matrix products, advance(): in_re = jnp.dot(grouped, push_re, precision=HIGHEST)  15.3 us
  transfers between devices with their start and end apart: 3, of which 2 were waited for; matrix products, arithmetic and copies ran while one was open for 3% of the time, Pallas kernels for 0%

profile of v1, /device:TPU:33, one launch (start us, length us, event | category | flops | bytes accessed | tf_op | source)
XLA Modules:
  0.0 368.5 jit_solution(6470050445651395024)
XLA Ops:
  5.9 4.2 %collective-permute-start = (bf16[256,2048]{1,0:T(8,128)(2,1)}, bf16[256,2048]{1,0:T(8,128)(2,1)}, u32[]{:S(2)}, u32[]{:S(2)}) collective-permute-start(bf16[256,2048]{1,0:T(8,128)(2,1)} %get-tuple-element.651), channel_id=1, source_target_pairs={{0,1},{1,2},{2,3},{3,0},{4,5},{5,6},{6,7},{7,4},{8,9},{9,10},{10,1... | collective-permute-start | bytes 3145736 | tf_op jit(solution)/shard_map/ppermute | solution.py:19
  10.1 3.5 collective-permute-start.1
  16.5 7.6 %collective-permute-done = bf16[256,2048]{1,0:T(8,128)(2,1)} collective-permute-done((bf16[256,2048]{1,0:T(8,128)(2,1)}, bf16[256,2048]{1,0:T(8,128)(2,1)}, u32[]{:S(2)}, u32[]{:S(2)}) %collective-permute-start) | collective-permute-done | bytes 1048608 | tf_op jit(solution)/shard_map/ppermute | solution.py:19
  24.1 11.5 %collective-permute-start.2 = (bf16[256,2048]{1,0:T(8,128)(2,1)}, bf16[256,2048]{1,0:T(8,128)(2,1)}, u32[]{:S(2)}, u32[]{:S(2)}) collective-permute-start(bf16[256,2048]{1,0:T(8,128)(2,1)} %collective-permute-done), channel_id=1, source_target_pairs={{0,1},{1,2},{2,3},{3,0},{4,5},{5,6},{6,7},{7,4},{8,9},{9,10},{10,1... | collective-permute-start | bytes 3145736 | tf_op jit(solution)/shard_map/ppermute | solution.py:19
  42.3 8.2 %collective-permute-done.2 = bf16[256,2048]{1,0:T(8,128)(2,1)} collective-permute-done((bf16[256,2048]{1,0:T(8,128)(2,1)}, bf16[256,2048]{1,0:T(8,128)(2,1)}, u32[]{:S(2)}, u32[]{:S(2)}) %collective-permute-start.2) | collective-permute-done | bytes 1048608 | tf_op jit(solution)/shard_map/ppermute | solution.py:19
  52.8 4.1 %convolution_convert_fusion.1 = bf16[1024,128]{1,0:T(8,128)(2,1)} fusion(bf16[1024,2048]{1,0:T(8,128)(2,1)} %constant_dynamic-update-slice_fusion, bf16[2048,128]{1,0:T(8,128)(2,1)S(1)} %copy-done.18), kind=kOutput, calls=%fused_computation.81 | convolution fusion | flops 537001984 | bytes 4980736 | tf_op jit(solution)/shard_map/dot_general | solution.py:144
  58.1 174.6 %while.48 = (s32[]{:T(128)}, f32[512]{0:T(512)S(1)}, f32[512]{0:T(512)S(1)}, f32[512]{0:T(512)}, f32[512]{0:T(512)}, /*index=5*/f32[16,64,512]{2,1,0:T(8,128)}, ...) while((s32[]{:T(128)}, f32[512]{0:T(512)S(1)}, ...), condition=%wide.wide.region_2.3_spmd.clone.clone.clone, body=%wide.wide.region_1.2_spmd.clone.clone.clone.sunk | while | flops 153889792 | bytes 4405837 | solution.py:161
  64.3 3.0 add_dynamic-update-slice_fusion.3
  75.2 3.0 add_dynamic-update-slice_fusion.3
  86.1 3.0 add_dynamic-update-slice_fusion.3
  97.0 3.0 add_dynamic-update-slice_fusion.3
  129.7 3.0 add_dynamic-update-slice_fusion.3
  140.6 3.0 add_dynamic-update-slice_fusion.3
  151.5 3.0 add_dynamic-update-slice_fusion.3
  162.4 3.0 add_dynamic-update-slice_fusion.3
  173.4 3.0 add_dynamic-update-slice_fusion.3
  195.2 3.0 add_dynamic-update-slice_fusion.3
  206.1 3.0 add_dynamic-update-slice_fusion.3
  217.0 3.0 add_dynamic-update-slice_fusion.3
  227.9 3.0 add_dynamic-update-slice_fusion.3
  233.4 110.3 %all-gather.1 = f32[64,4,512]{2,1,0:T(4,128)S(1)} all-gather(f32[1,4,512]{2,1,0:T(4,128)S(1)} %maximum_bitcast_fusion), channel_id=2, replica_groups=mesh['grp'=2,'sp'=64,'tp'=4] {'sp'}, dimensions={0}, use_global_device_ids=true | all-gather | bytes 532480 | tf_op jit(solution)/shard_map/all_gather | solution.py:37
  344.2 5.1 %while.47 = (s32[]{:T(128)}, f32[512]{0:T(512)S(1)}, f32[512]{0:T(512)S(1)}, s32[]{:T(128)}, f32[64,512]{1,0:T(8,128)S(1)}, /*index=5*/f32[64,512]{1,0:T(8,128)S...) while((s32[]{:T(128)}, f32[512]{0:T(512)S(1)}, f32[512]{0:T(512)S(1)}, ...), condition=%wide.region_4.5_spmd.clone, body=%wide.region_3.4_spmd.clone.sunk | while | flops 6148 | bytes 32897 | solution.py:57
  349.3 4.6 %multiply_add_fusion.5 = (f32[16,64,512]{2,1,0:T(8,128)S(1)}, f32[16,64,512]{2,1,0:T(8,128)S(1)}) fusion(f32[16,64,512]{2,1,0:T(8,128)} %get-tuple-element.435, f32[16,64,512]{2,1,0:T(8,128)} %get-tuple-element.437, f32[16,64,512]{2,1,0:T(8,128)} %get-tuple-element.429, f32[512]{0:T(512)S(1)} %get-tuple-element.436, f32[512]{0:T(512)S(1)} %get-tuple-element.434, ...), kind=kLoop, calls=%fused_computation.78 | loop fusion | flops 4194304 | bytes 12587008 | tf_op jit(solution)/shard_map/add | solution.py:174
  357.7 8.9 %all_to_all.13 = bf16[4,256,128]{1,2,0:T(8,128)(2,1)S(1)} all-to-all(bf16[4,256,128]{1,2,0:T(8,128)(2,1)S(1)} %copy.20), channel_id=1, replica_groups=mesh['grp'=2,'sp'=64,'tp'=4] {'tp'}, dimensions={0} | all-to-all | bytes 524288 | tf_op jit(solution)/shard_map/all_to_all | solution.py:176
  (648 shorter events, 161.1 us)
Async XLA Ops:
  0.0 366.8 %copy-start = (bf16[512,2048]{1,0:T(8,128)(2,1)S(1)}, bf16[512,2048]{1,0:T(8,128)(2,1)}, u32[]{:S(2)}) copy-start(bf16[512,2048]{1,0:T(8,128)(2,1)} %param.23) | copy-start | bytes 6291460
  4.2 9.5 %copy-start.9 = (f32[8,64]{1,0:T(8,128)S(1)}, f32[8,64]{1,0:T(8,128)}, u32[]{:S(2)}) copy-start(f32[8,64]{1,0:T(8,128)} %param.19) | copy-start | bytes 6148
  4.2 9.6 %copy-start.10 = (f32[8,64]{1,0:T(8,128)S(1)}, f32[8,64]{1,0:T(8,128)}, u32[]{:S(2)}) copy-start(f32[8,64]{1,0:T(8,128)} %param.18) | copy-start | bytes 6148
  4.2 11.6 %copy-start.14 = (f32[1024]{0:T(1024)S(1)}, f32[1024]{0:T(1024)}, u32[]{:S(2)}) copy-start(f32[1024]{0:T(1024)} %param.15) | copy-start | bytes 12292
  4.2 12.3 %copy-start.4 = (f32[2,8,16,64]{3,2,1,0:T(8,128)S(1)}, f32[2,8,16,64]{3,2,1,0:T(8,128)}, u32[]{:S(2)}) copy-start(f32[2,8,16,64]{3,2,1,0:T(8,128)} %param.21) | copy-start | bytes 196612
  5.9 31.7 %copy-start.5 = (f32[2,8,64,16]{2,3,1,0:T(8,128)S(1)}, f32[2,8,64,16]{2,3,1,0:T(8,128)}, u32[]{:S(2)}) copy-start(f32[2,8,64,16]{2,3,1,0:T(8,128)} %param.20) | copy-start | bytes 196612
  5.9 18.3 %collective-permute-start = (bf16[256,2048]{1,0:T(8,128)(2,1)}, bf16[256,2048]{1,0:T(8,128)(2,1)}, u32[]{:S(2)}, u32[]{:S(2)}) collective-permute-start(bf16[256,2048]{1,0:T(8,128)(2,1)} %get-tuple-element.651), channel_id=1, source_target_pairs={{0,1},{1,2},{2,3},{3,0},{4,5},{5,6},{6,7},{7,4},{8,9},{9,10},{10,1... | collective-permute-start | bytes 3145736 | tf_op jit(solution)/shard_map/ppermute | solution.py:19
  10.1 29.9 %collective-permute-start.1 = (bf16[256,2048]{1,0:T(8,128)(2,1)}, bf16[256,2048]{1,0:T(8,128)(2,1)}, u32[]{:S(2)}, u32[]{:S(2)}) collective-permute-start(bf16[256,2048]{1,0:T(8,128)(2,1)} %get-tuple-element.651), channel_id=1, source_target_pairs={{0,3},{1,0},{2,1},{3,2},{4,7},{5,4},{6,5},{7,6},{8,11},{9,8},{10,9... | collective-permute-start | bytes 3145736 | tf_op jit(solution)/shard_map/ppermute | solution.py:22
  24.1 26.3 %collective-permute-start.2 = (bf16[256,2048]{1,0:T(8,128)(2,1)}, bf16[256,2048]{1,0:T(8,128)(2,1)}, u32[]{:S(2)}, u32[]{:S(2)}) collective-permute-start(bf16[256,2048]{1,0:T(8,128)(2,1)} %collective-permute-done), channel_id=1, source_target_pairs={{0,1},{1,2},{2,3},{3,0},{4,5},{5,6},{6,7},{7,4},{8,9},{9,10},{10,1... | collective-permute-start | bytes 3145736 | tf_op jit(solution)/shard_map/ppermute | solution.py:19
  39.9 12.9 %copy-start.18 = (bf16[2048,128]{1,0:T(8,128)(2,1)S(1)}, bf16[2048,128]{1,0:T(8,128)(2,1)}, u32[]{:S(2)}) copy-start(bf16[2048,128]{1,0:T(8,128)(2,1)} %param.17) | copy-start | bytes 1572868
  145.7 5.8 %copy-start.6 = (f32[1,512]{1,0:T(1,128)S(1)}, f32[1,512]{1,0:T(1,128)}, u32[]{:S(2)}) copy-start(f32[1,512]{1,0:T(1,128)} %get-tuple-element.1030) | copy-start | bytes 6148 | tf_op jit(solution)/shard_map/while
  145.7 5.8 %copy-start.12 = (f32[512]{0:T(512)S(1)}, f32[512]{0:T(512)}, u32[]{:S(2)}) copy-start(f32[512]{0:T(512)} %get-tuple-element.1003) | copy-start | bytes 6148 | tf_op jit(solution)/shard_map/while
  145.7 5.8 %copy-start.13 = (f32[512]{0:T(512)S(1)}, f32[512]{0:T(512)}, u32[]{:S(2)}) copy-start(f32[512]{0:T(512)} %get-tuple-element.1004) | copy-start | bytes 6148 | tf_op jit(solution)/shard_map/while
  145.7 5.8 %copy-start.16 = (f32[512]{0:T(512)S(1)}, f32[512]{0:T(512)}, u32[]{:S(2)}) copy-start(f32[512]{0:T(512)} %get-tuple-element.1040) | copy-start | bytes 6148 | tf_op jit(solution)/shard_map/while
  145.8 5.8 %copy-start.17 = (f32[1,512]{1,0:T(1,128)S(1)}, f32[1,512]{1,0:T(1,128)}, u32[]{:S(2)}) copy-start(f32[1,512]{1,0:T(1,128)} %get-tuple-element.1034) | copy-start | bytes 6148 | tf_op jit(solution)/shard_map/while
  167.5 5.8 %copy-start.6 = (f32[1,512]{1,0:T(1,128)S(1)}, f32[1,512]{1,0:T(1,128)}, u32[]{:S(2)}) copy-start(f32[1,512]{1,0:T(1,128)} %get-tuple-element.1030) | copy-start | bytes 6148 | tf_op jit(solution)/shard_map/while
  167.5 5.8 %copy-start.12 = (f32[512]{0:T(512)S(1)}, f32[512]{0:T(512)}, u32[]{:S(2)}) copy-start(f32[512]{0:T(512)} %get-tuple-element.1003) | copy-start | bytes 6148 | tf_op jit(solution)/shard_map/while
  167.6 5.8 %copy-start.13 = (f32[512]{0:T(512)S(1)}, f32[512]{0:T(512)}, u32[]{:S(2)}) copy-start(f32[512]{0:T(512)} %get-tuple-element.1004) | copy-start | bytes 6148 | tf_op jit(solution)/shard_map/while
  167.6 5.8 %copy-start.16 = (f32[512]{0:T(512)S(1)}, f32[512]{0:T(512)}, u32[]{:S(2)}) copy-start(f32[512]{0:T(512)} %get-tuple-element.1040) | copy-start | bytes 6148 | tf_op jit(solution)/shard_map/while
  167.6 5.8 %copy-start.17 = (f32[1,512]{1,0:T(1,128)S(1)}, f32[1,512]{1,0:T(1,128)}, u32[]{:S(2)}) copy-start(f32[1,512]{1,0:T(1,128)} %get-tuple-element.1034) | copy-start | bytes 6148 | tf_op jit(solution)/shard_map/while
  211.2 5.8 %copy-start.6 = (f32[1,512]{1,0:T(1,128)S(1)}, f32[1,512]{1,0:T(1,128)}, u32[]{:S(2)}) copy-start(f32[1,512]{1,0:T(1,128)} %get-tuple-element.1030) | copy-start | bytes 6148 | tf_op jit(solution)/shard_map/while
  232.7 111.4 %copy-start.7 = (f32[512]{0:T(512)S(1)}, f32[512]{0:T(512)}, u32[]{:S(2)}) copy-start(f32[512]{0:T(512)} %custom-call) | copy-start | bytes 6148
  232.7 111.4 %copy-start.8 = (f32[512]{0:T(512)S(1)}, f32[512]{0:T(512)}, u32[]{:S(2)}) copy-start(f32[512]{0:T(512)} %custom-call.1) | copy-start | bytes 6148
  355.7 11.0 %copy-start.15 = (f32[512]{0:T(512)S(1)}, f32[512]{0:T(512)}, u32[]{:S(2)}) copy-start(f32[512]{0:T(512)} %param.22) | copy-start | bytes 6148
  (73 other events, 409.2 us)
